TPU v7x, 32 devices: a whole 2x2x4 slice. The times are simulated.
32 devices in a mesh: ra: 4 (over z), cb: 8 (over y, x, core).
Axes of the slice: x: 2, y: 2, z: 4, core: 2. Of those that a mesh axis runs over, the one named last changes fastest.
Arguments:
- tokens: bfloat16 [512, 3072], P(None, 'ra'), may hold values from -14 to 14
- norm_gain: float32 [2, 3072], P(None, 'ra'), may hold values from 0.1 to 1.9
- gate_weight: float32 [2, 3072, 8448], P(None, 'ra', 'cb'), may hold values from -0.109375 to 0.109375
- gate_scale: float32 [2, 8448], P(None, 'cb'), may hold values from 0.5 to 2
- value_weight: float32 [2, 3072, 8448], P(None, 'ra', 'cb'), may hold values from -0.109375 to 0.109375
- value_scale: float32 [2, 8448], P(None, 'cb'), may hold values from 0.5 to 2
- gate_conv: float32 [2, 3, 8448], P(None, None, 'cb'), may hold values from -3.5 to 3.5
- value_conv: float32 [2, 3, 8448], P(None, None, 'cb'), may hold values from -3.5 to 3.5
- gate_bias: float32 [2, 8448], P(None, 'cb'), may hold values from -3 to 3
- value_bias: float32 [2, 8448], P(None, 'cb'), may hold values from -3 to 3
- down_weight: float32 [2, 8448, 3072], P(None, 'cb', 'ra'), may hold values from -0.0625 to 0.0625
- down_scale: float32 [2, 3072], P(None, 'ra'), may hold values from 0.5 to 2
Outputs:
- stream_out: bfloat16 [512, 3072], P(None, 'ra')
All inputs are finite; a program needn't handle non-finite values.
Results may differ from a plain program's by a relative error of at most 0.039.
Values may be sent and summed in bfloat16 or wider, within the bound.
A program may use at most 64 MiB of HBM per device.

v0:
```python
import jax
import jax.numpy as jnp
from jax import lax
from jax.sharding import PartitionSpec as P

D = 3072
TAPS = 3
LAYERS = 2
SEQ_LEN = 8


epsilon = 1e-06
residual_keep = 0.5


def causal_conv(values, conv_taps, conv_bias):
    row_count, col_count = values.shape
    blocks = values.reshape(row_count // SEQ_LEN, SEQ_LEN, col_count)
    padded = jnp.pad(blocks, ((0, 0), (TAPS - 1, 0), (0, 0)))
    summed = conv_bias + jnp.zeros_like(blocks)
    for offset in range(TAPS):
        summed = summed + padded[:, offset : offset + SEQ_LEN] * conv_taps[offset]
    return summed.reshape(row_count, col_count)


def shards(
    tokens,
    norm_gain,
    gate_weight,
    gate_scale,
    value_weight,
    value_scale,
    gate_conv,
    value_conv,
    gate_bias,
    value_bias,
    down_weight,
    down_scale,
):
    stream = tokens
    for depth_index in range(LAYERS):
        widened = stream.astype(jnp.float32)
        local_squares = jnp.sum(widened * widened, axis=1)
        normed = (widened * norm_gain[depth_index]).astype(jnp.bfloat16)
        gate_part = jnp.dot(
            normed,
            gate_weight[depth_index].astype(jnp.bfloat16),
            preferred_element_type=jnp.float32,
        )
        value_part = jnp.dot(
            normed,
            value_weight[depth_index].astype(jnp.bfloat16),
            preferred_element_type=jnp.float32,
        )
        squares, gate_pre, value_pre = (
            lax.psum_scatter(
                local_squares.astype(jnp.bfloat16), "ra", scatter_dimension=0, tiled=True
            ).astype(jnp.float32),
            lax.psum_scatter(
                gate_part.astype(jnp.bfloat16), "ra", scatter_dimension=0, tiled=True
            ).astype(jnp.float32),
            lax.psum_scatter(
                value_part.astype(jnp.bfloat16), "ra", scatter_dimension=0, tiled=True
            ).astype(jnp.float32),
        )
        inverse_rms = lax.rsqrt(squares / D + epsilon)[:, None]
        gate_mixed = causal_conv(
            gate_pre * inverse_rms * gate_scale[depth_index],
            gate_conv[depth_index],
            gate_bias[depth_index],
        )
        value_mixed = causal_conv(
            value_pre * inverse_rms * value_scale[depth_index],
            value_conv[depth_index],
            value_bias[depth_index],
        )
        hidden = (jax.nn.silu(gate_mixed) * value_mixed).astype(jnp.bfloat16)
        hidden = lax.all_gather(hidden, "ra", axis=0, tiled=True)
        partial_value = jnp.dot(
            hidden,
            down_weight[depth_index].astype(jnp.bfloat16),
            preferred_element_type=jnp.float32,
        )
        branch = (
            lax.psum(partial_value.astype(jnp.bfloat16), "cb").astype(jnp.float32)
            * down_scale[depth_index]
        )
        stream = (residual_keep * widened + branch).astype(jnp.bfloat16)
    return stream


def solution(mesh):
    placed = (
        P(None, "ra"),
        P(None, "ra"),
        P(None, "ra", "cb"),
        P(None, "cb"),
        P(None, "ra", "cb"),
        P(None, "cb"),
        P(None, None, "cb"),
        P(None, None, "cb"),
        P(None, "cb"),
        P(None, "cb"),
        P(None, "cb", "ra"),
        P(None, "ra"),
    )
    return jax.shard_map(
        shards, mesh=mesh, in_specs=placed, out_specs=P(None, "ra"), check_vma=False
    )
```

profile of v0, /device:TPU:0, one launch (start us, length us, event | category | flops | bytes accessed | tf_op | source)
XLA Modules:
  0.0 335.4 jit_solution(7791653706815640142)
XLA Ops:
  6.5 0.0 reduce-scatter.13.cloned.1.call-start
  6.5 0.8 slice_reduce_fusion.21
  7.3 0.0 copy-start.2
  7.3 3.2 convert.12
  10.6 2.1 convolution_convert_fusion.3
  12.7 2.4 copy.21
  15.0 0.0 reduce-scatter.13.cloned.1.call-update
  15.0 0.0 reduce-scatter.15.cloned.1.call-start
  15.1 0.0 copy-start.3
  15.1 3.2 convert.13
  18.3 1.7 copy-done
  20.0 2.1 convolution_convert_fusion.2
  22.1 2.4 copy.23
  24.5 0.0 reduce-scatter.15.cloned.1.call-update
  24.6 0.0 all-gather.3.cloned.1.call-start
  24.6 0.6 dynamic-slice
  25.9 1.4 fusion.5
  27.2 14.0 %all-reduce.4 = bf16[512]{0:T(512)(128)(2,1)S(1)} all-reduce(bf16[512]{0:T(512)(128)(2,1)S(1)} %fusion.5), channel_id=3, replica_groups=mesh['ra'=4,'cb'=8] {'ra'}, use_global_device_ids=true, to_apply=%region_2.0.clone | all-reduce | flops 512 | bytes 2048
  41.2 0.1 fusion.48
  41.3 0.0 copy-done.7
  41.3 0.1 slice_reduce_fusion.3
  41.4 0.0 copy-done.9
  41.4 0.0 copy-done.10
  41.4 0.1 slice_reduce_fusion.4
  41.5 0.0 copy-done.5
  41.5 0.0 copy-done.6
  41.5 0.1 slice_reduce_fusion.2
  41.6 5.9 %reduce-scatter.13.cloned.1.call-done = bf16[128,1056]{1,0:T(8,128)(2,1)} async-done(((bf16[512,1056]{1,0:T(8,128)(2,1)}), bf16[128,1056]{1,0:T(8,128)(2,1)}) %reduce-scatter.13.cloned.1.call-update) | async-done | bytes 270352 | tf_op jit(solution)/shard_map/reduce_scatter | solution.py:59
  47.5 30.2 %reduce-scatter.15.cloned.1.call-done = bf16[128,1056]{1,0:T(8,128)(2,1)} async-done(((bf16[512,1056]{1,0:T(8,128)(2,1)}), bf16[128,1056]{1,0:T(8,128)(2,1)}) %reduce-scatter.15.cloned.1.call-update) | async-done | bytes 270352 | tf_op jit(solution)/shard_map/reduce_scatter | solution.py:62
  77.8 1.2 multiply_bitcast_fusion.3
  79.0 1.2 fusion.28
  80.2 0.0 all-gather.3.cloned.1.call-update
  80.3 0.0 all-reduce.9.cloned.1.call-start
  80.3 4.8 %convert.14 = bf16[2,1056,768]{2,1,0:T(8,128)(2,1)} convert(f32[2,1056,768]{2,1,0:T(8,128)} %param.22) | non-fusion elementwise | flops 1622016 | bytes 9732096 | tf_op jit(solution)/shard_map/convert.3
  85.2 24.1 %all-gather.3.cloned.1.call-done = bf16[512,1056]{1,0:T(8,128)(2,1)} async-done(((bf16[128,1056]{1,0:T(8,128)(2,1)}), bf16[512,1056]{1,0:T(8,128)(2,1)}) %all-gather.3.cloned.1.call-update) | async-done | bytes 1081360 | tf_op jit(solution)/shard_map/all_gather | solution.py:78
  109.3 3.9 %fusion.10 = bf16[512,768]{1,0:T(8,128)(2,1)} fusion(bf16[512,1056]{1,0:T(8,128)(2,1)} %all-gather.3.cloned.1.call-done, bf16[2,1056,768]{2,1,0:T(8,128)(2,1)} %convert.14), kind=kOutput, calls=%fused_computation.34 | convolution fusion | flops 830865408 | bytes 3588096 | tf_op jit(solution)/shard_map/dot_general | solution.py:79
  113.1 0.0 all-reduce.9.cloned.1.call-update
  113.2 0.0 reduce-scatter.19.cloned.1.call-start
  113.3 55.0 %all-reduce.9.cloned.1.call-done = bf16[512,768]{1,0:T(8,128)(2,1)} async-done(((bf16[512,768]{1,0:T(8,128)(2,1)}), bf16[512,768]{1,0:T(8,128)(2,1)}) %all-reduce.9.cloned.1.call-update) | async-done | bytes 786448 | tf_op jit(solution)/shard_map/psum | solution.py:85
  168.2 1.8 fusion.9
  170.0 0.0 copy-start.4
  170.0 0.9 copy-done.4
  170.9 3.5 %convolution_convert_fusion = bf16[512,1056]{0,1:T(8,128)(2,1)} fusion(bf16[2,768,1056]{1,2,0:T(8,128)(2,1)} %copy-done, bf16[512,768]{1,0:T(8,128)(2,1)S(1)} %get-tuple-element.30, f32[768]{0:T(1024)S(1)} %get-tuple-element.27), kind=kOutput, calls=%fused_computation | convolution fusion | flops 832192512 | bytes 3492864 | tf_op jit(solution)/shard_map/dot_general | solution.py:50
  174.4 2.3 copy.27
  176.8 0.0 reduce-scatter.19.cloned.1.call-update
  176.8 0.0 reduce-scatter.17.cloned.1.call-start
  176.8 3.2 convolution_convert_fusion.1
  180.0 2.4 copy.25
  182.4 0.0 reduce-scatter.17.cloned.1.call-update
  182.4 0.0 all-gather.5.cloned.1.call-start
  182.4 12.0 %all-reduce.5 = bf16[512]{0:T(512)(128)(2,1)S(1)} all-reduce(bf16[512]{0:T(512)(128)(2,1)S(1)} %get-tuple-element.29), channel_id=6, replica_groups=mesh['ra'=4,'cb'=8] {'ra'}, use_global_device_ids=true, to_apply=%region_7.8.clone | all-reduce | flops 512 | bytes 2048
  194.5 0.1 fusion.49
  194.6 11.3 %reduce-scatter.19.cloned.1.call-done = bf16[128,1056]{1,0:T(8,128)(2,1)} async-done(((bf16[512,1056]{1,0:T(8,128)(2,1)}), bf16[128,1056]{1,0:T(8,128)(2,1)}) %reduce-scatter.19.cloned.1.call-update) | async-done | bytes 270352 | tf_op jit(solution)/shard_map/reduce_scatter | solution.py:62
  205.8 30.1 %reduce-scatter.17.cloned.1.call-done = bf16[128,1056]{1,0:T(8,128)(2,1)} async-done(((bf16[512,1056]{1,0:T(8,128)(2,1)}), bf16[128,1056]{1,0:T(8,128)(2,1)}) %reduce-scatter.17.cloned.1.call-update) | async-done | bytes 270352 | tf_op jit(solution)/shard_map/reduce_scatter | solution.py:59
  235.9 1.4 multiply_bitcast_fusion.1
  237.3 1.2 fusion.42
  238.6 0.0 all-gather.5.cloned.1.call-update
  238.6 0.0 all-reduce.11.cloned.1.call-start
  238.6 29.0 %all-gather.5.cloned.1.call-done = bf16[512,1056]{1,0:T(8,128)(2,1)} async-done(((bf16[128,1056]{1,0:T(8,128)(2,1)}), bf16[512,1056]{1,0:T(8,128)(2,1)}) %all-gather.5.cloned.1.call-update) | async-done | bytes 1081360 | tf_op jit(solution)/shard_map/all_gather | solution.py:78
  267.6 0.0 copy-done.1
  267.6 3.3 fusion.11
  270.9 0.0 all-reduce.11.cloned.1.call-update
  271.0 55.0 %all-reduce.11.cloned.1.call-done = bf16[512,768]{1,0:T(8,128)(2,1)} async-done(((bf16[512,768]{1,0:T(8,128)(2,1)}), bf16[512,768]{1,0:T(8,128)(2,1)}) %all-reduce.11.cloned.1.call-update) | async-done | bytes 786448 | tf_op jit(solution)/shard_map/psum | solution.py:85
  326.0 2.5 fusion.7
  (16 shorter events, 0.0 us)
Async XLA Ops:
  6.5 41.0 %reduce-scatter.13.cloned.1.call-start = ((), (), s32[]{:S(2)}) async-start(), calls=%async_computation.8 | async-start | bytes 1474560 | tf_op jit(solution)/shard_map/reduce_scatter | solution.py:59
  7.3 3.2 copy-start.2
  15.0 62.7 %reduce-scatter.15.cloned.1.call-start = ((), (), s32[]{:S(2)}) async-start(), calls=%async_computation.9 | async-start | bytes 1474560 | tf_op jit(solution)/shard_map/reduce_scatter | solution.py:62
  15.1 5.0 %copy-start.3 = (bf16[512,768]{1,0:T(8,128)(2,1)S(1)}, bf16[512,768]{1,0:T(8,128)(2,1)}, u32[]{:S(2)}) copy-start(bf16[512,768]{1,0:T(8,128)(2,1)} %param.12) | copy-start | bytes 2359300
  18.3 1.7 copy-start
  22.1 2.5 copy-start.12
  22.1 19.2 %copy-start.7 = (f32[2,1056]{1,0:T(2,128)S(1)}, f32[2,1056]{1,0:T(2,128)}, u32[]{:S(2)}) copy-start(f32[2,1056]{1,0:T(2,128)} %param.17) | copy-start | bytes 25348
  22.1 19.2 %copy-start.8 = (f32[2,1056]{1,0:T(2,128)S(1)}, f32[2,1056]{1,0:T(2,128)}, u32[]{:S(2)}) copy-start(f32[2,1056]{1,0:T(2,128)} %param.15) | copy-start | bytes 25348
  24.5 16.8 %copy-start.9 = (f32[2,1056]{1,0:T(2,128)S(1)}, f32[2,1056]{1,0:T(2,128)}, u32[]{:S(2)}) copy-start(f32[2,1056]{1,0:T(2,128)} %param.21) | copy-start | bytes 25348
  24.5 16.9 %copy-start.10 = (f32[2,1056]{1,0:T(2,128)S(1)}, f32[2,1056]{1,0:T(2,128)}, u32[]{:S(2)}) copy-start(f32[2,1056]{1,0:T(2,128)} %param.20) | copy-start | bytes 25348
  24.5 16.9 %copy-start.5 = (f32[2,3,1056]{2,0,1:T(2,128)S(1)}, f32[2,3,1056]{2,0,1:T(2,128)}, u32[]{:S(2)}) copy-start(f32[2,3,1056]{2,0,1:T(2,128)} %param.19) | copy-start | bytes 76036
  24.5 16.9 %copy-start.6 = (f32[2,3,1056]{2,0,1:T(2,128)S(1)}, f32[2,3,1056]{2,0,1:T(2,128)}, u32[]{:S(2)}) copy-start(f32[2,3,1056]{2,0,1:T(2,128)} %param.18) | copy-start | bytes 76036
  24.6 84.7 %all-gather.3.cloned.1.call-start = ((), (), s32[]{:S(2)}) async-start(), calls=%async_computation.4 | async-start | bytes 1474560 | tf_op jit(solution)/shard_map/all_gather | solution.py:78
  80.3 87.9 %all-reduce.9.cloned.1.call-start = ((), (), s32[]{:S(2)}) async-start(), calls=%async_computation.5 | async-start | bytes 1572864 | tf_op jit(solution)/shard_map/psum | solution.py:85
  85.2 28.1 %copy-start.11 = (f32[2,768]{1,0:T(2,128)S(1)}, f32[2,768]{1,0:T(2,128)}, u32[]{:S(2)}) copy-start(f32[2,768]{1,0:T(2,128)} %param.23) | copy-start | bytes 18436
  113.2 92.7 %reduce-scatter.19.cloned.1.call-start = ((), (), s32[]{:S(2)}) async-start(), calls=%async_computation.11 | async-start | bytes 1474560 | tf_op jit(solution)/shard_map/reduce_scatter | solution.py:62
  170.0 0.9 copy-start.4
  176.8 59.2 %reduce-scatter.17.cloned.1.call-start = ((), (), s32[]{:S(2)}) async-start(), calls=%async_computation.10 | async-start | bytes 1474560 | tf_op jit(solution)/shard_map/reduce_scatter | solution.py:59
  182.4 85.2 %all-gather.5.cloned.1.call-start = ((), (), s32[]{:S(2)}) async-start(), calls=%async_computation.6 | async-start | bytes 1474560 | tf_op jit(solution)/shard_map/all_gather | solution.py:78
  235.9 31.7 %copy-start.1 = (bf16[2,1056,768]{2,1,0:T(8,128)(2,1)S(1)}, bf16[2,1056,768]{2,1,0:T(8,128)(2,1)}, u32[]{:S(2)}) copy-start(bf16[2,1056,768]{2,1,0:T(8,128)(2,1)} %convert.14) | copy-start | bytes 9732100
  238.6 87.4 %all-reduce.11.cloned.1.call-start = ((), (), s32[]{:S(2)}) async-start(), calls=%async_computation.7 | async-start | bytes 1572864 | tf_op jit(solution)/shard_map/psum | solution.py:85
Sparse Core Ops, SparseCore 0:
  15.2 32.3 reduce-scatter.12
  49.8 27.8 reduce-scatter.14
  80.4 28.8 all-gather.2
  113.3 54.8 all-reduce.8
  176.9 28.8 reduce-scatter.18
  208.0 27.8 reduce-scatter.16
  238.7 28.8 all-gather.4
  271.1 54.8 all-reduce.10
where the time goes:
time: 336 us; the launch traced here: 335 us
  waiting for transfers between devices  241 us (72%)
  blocking collectives  26 us (8%)
  other arithmetic  22.3 us (7%)
  matrix products  18 us (5%)
  between operations  14.3 us (4%)
  local copies, waits for them, and re-layouts  13.7 us (4%)
    psum x2, waiting for transfers between devices, shards(): lax.psum(partial_value.astype(jnp.bfloat16), 'cb').astype(jnp.float32)  110 us
    all_gather x2, waiting for transfers between devices, shards(): hidden = lax.all_gather(hidden, 'ra', axis=0, tiled=True)  53.1 us
    reduce_scatter x2, waiting for transfers between devices, shards(): lax.psum_scatter(value_part.astype(jnp.bfloat16), 'ra', scatter_dimension...  41.5 us
    reduce_scatter x2, waiting for transfers between devices, shards(): lax.psum_scatter(gate_part.astype(jnp.bfloat16), 'ra', scatter_dimension=...  36 us
    unnamed x2, blocking collectives  26 us
    unnamed x31, local copies, waits for them, and re-layouts  12.7 us
    another operation x3, other arithmetic  11.3 us
    dot_general x2, matrix products, shards(): jnp.dot(hidden, down_weight[depth_index].astype(jnp.bfloat16), preferred_...  7.18 us
  transfers between devices with their start and end apart: 8, of which 8 were waited for; matrix products, arithmetic and copies ran while one was open for 6% of the time, Pallas kernels for 0%

commit v1 on v0

v1 whole, which is shorter than its diff:
```python
import functools
import jax
import jax.numpy as jnp
from jax import lax
from jax.experimental import pallas as pl
from jax.experimental.pallas import tpu as pltpu
from jax.sharding import PartitionSpec as P

SEQ_LEN = 8
EPSILON = 1e-06
RESIDUAL_KEEP = 0.5
MESH = pl.DeviceIdType.MESH
LANES = 128


def kernel(
    cfg,
    tokens_ref,
    gain_ref,
    gw_ref,
    gs_ref,
    vw_ref,
    vs_ref,
    gc_ref,
    vc_ref,
    gb_ref,
    vb_ref,
    dw_ref,
    ds_ref,
    out_ref,
    stage_g,
    stage_v,
    stage_d,
    wc,
    wd,
    par,
    xs,
    own,
    pin,
    pout,
    hid,
    ro,
    ri,
    w_sem,
    ps,
    pr,
    hs,
    hr,
    rs_s,
    rs_r,
    ag_s,
    ag_r,
):
    R, N, L, n, m, D, F = cfg
    Dl = tokens_ref.shape[1]
    rows = 2 * m
    own_rows = rows // N
    taps = gc_ref.shape[1]
    full = F // LANES * LANES
    rest = F - full
    wide = full + LANES
    sq_lane = 2 * rest
    S = max(n, 2 * R)
    z = lax.axis_index("ra")
    me = lax.axis_index("cb")

    def weight_copies(l):
        return (
            pltpu.make_async_copy(gw_ref.at[l], stage_g, w_sem.at[0]),
            pltpu.make_async_copy(vw_ref.at[l], stage_v, w_sem.at[1]),
            pltpu.make_async_copy(dw_ref.at[l], stage_d, w_sem.at[2]),
        )

    for copy in weight_copies(0):
        copy.start()

    barrier = pltpu.get_barrier_semaphore()
    for k in range(1, N):
        pl.semaphore_signal(
            barrier, inc=1, device_id={"cb": lax.rem(me + k, N)}, device_id_type=MESH
        )

    @pl.when(z > 0)
    def _():
        pl.semaphore_signal(barrier, inc=1, device_id={"ra": z - 1}, device_id_type=MESH)

    @pl.when(z < R - 1)
    def _():
        pl.semaphore_signal(barrier, inc=1, device_id={"ra": z + 1}, device_id_type=MESH)

    for i in range(n):
        block = tokens_ref[i * rows : (i + 1) * rows, :].astype(jnp.float32)
        xs[i] = block.reshape(N, own_rows, Dl).astype(jnp.bfloat16)

    par[...] = jnp.zeros_like(par)
    for l in range(L):
        par[l, 0:1, 0:F] = gs_ref[l : l + 1, :]
        par[l, 1:2, 0:F] = vs_ref[l : l + 1, :]
        par[l, 2:3, 0:F] = gb_ref[l : l + 1, :]
        par[l, 3:4, 0:F] = vb_ref[l : l + 1, :]
        par[l, 4 : 4 + taps, 0:F] = gc_ref[l]
        par[l, 4 + taps : 4 + 2 * taps, 0:F] = vc_ref[l]

    def cast_weights(l):
        copies = weight_copies(l)
        copies[0].wait()
        copies[1].wait()

        def up(b, carry):
            at = pl.ds(pl.multiple_of(b * 32, 32), 32)
            wc[l, at, 0:full] = stage_g[at, 0:full].astype(jnp.bfloat16)
            wc[l, at, full : 2 * full] = stage_v[at, 0:full].astype(jnp.bfloat16)
            tail = jnp.concatenate(
                [
                    stage_g[at, full:F],
                    stage_v[at, full:F],
                    jnp.zeros((32, LANES - 2 * rest), jnp.float32),
                ],
                axis=1,
            )
            wc[l, at, 2 * full : 2 * full + LANES] = tail.astype(jnp.bfloat16)
            return carry

        lax.fori_loop(0, Dl // 32, up, 0)
        copies[2].wait()

        def down(b, carry):
            at = pl.ds(pl.multiple_of(b * 32, 32), 32)
            wd[l, at, :] = stage_d[at, :].astype(jnp.bfloat16)
            return carry

        lax.fori_loop(0, F // 32, down, 0)
        wd[l, F:wide, :] = jnp.zeros((wide - F, Dl), jnp.bfloat16)

    cast_weights(0)
    for l in range(1, L):
        for copy in weight_copies(l):
            copy.start()

    expected = N - 1 + jnp.where(z > 0, 1, 0) + jnp.where(z < R - 1, 1, 0)
    pl.semaphore_wait(barrier, expected)

    def when_item(g, fn):
        layer = lax.div(g, S)
        i = lax.rem(g, S)

        @pl.when((g >= 0) & (g < L * S) & (i < n))
        def _():
            fn(layer, i, layer * n + i)

    def part_copy(q, d, target):
        return pltpu.make_async_remote_copy(
            src_ref=pout.at[q, d],
            dst_ref=pin.at[q, d],
            send_sem=ps.at[q, d],
            recv_sem=pr.at[q, d],
            device_id={"ra": target},
            device_id_type=MESH,
        )

    def hid_copy(q, d, target):
        return pltpu.make_async_remote_copy(
            src_ref=hid.at[q, d],
            dst_ref=hid.at[q, d],
            send_sem=hs.at[q, d],
            recv_sem=hr.at[q, d],
            device_id={"ra": target},
            device_id_type=MESH,
        )

    row_in_seq = lax.rem(lax.broadcasted_iota(jnp.int32, (m, wide), 0), SEQ_LEN)
    lane = lax.broadcasted_iota(jnp.int32, (m, LANES), 1)

    def conv(values, l, first):
        total = values * par[l, first + taps - 1 : first + taps, :]
        for back in range(1, taps):
            moved = jnp.where(row_in_seq >= back, pltpu.roll(values, back, 0), 0.0)
            total = total + moved * par[l, first + taps - 1 - back : first + taps - back, :]
        return total

    def finish(l, q, d, main_g, main_v, tail):
        squares = jnp.sum(
            jnp.where((lane == sq_lane) | (lane == sq_lane + 1), tail, 0.0),
            axis=1,
            keepdims=True,
        )
        inverse = lax.rsqrt(squares / D + EPSILON)
        gate = jnp.concatenate([main_g, tail], axis=1)
        value = jnp.concatenate([main_v, pltpu.roll(tail, LANES - rest, 1)], axis=1)
        gate = gate * inverse * par[l, 0:1, :]
        value = value * inverse * par[l, 1:2, :]
        gate = par[l, 2:3, :] + conv(gate, l, 4)
        value = par[l, 3:4, :] + conv(value, l, 4 + taps)
        hid[q, d] = (gate / (1.0 + jnp.exp(-gate)) * value).astype(jnp.bfloat16)

    def chain(d, l, q):
        first = (z == 0) if d == 0 else (z == R - 1)
        last = (z == R - 1) if d == 0 else (z == 0)
        ahead = z + 1 if d == 0 else z - 1
        behind = z - 1 if d == 0 else z + 1

        def send(main_g, main_v, tail):
            squares = jnp.sum(
                jnp.where((lane == sq_lane) | (lane == sq_lane + 1), tail, 0.0),
                axis=1,
                keepdims=True,
            )
            high = squares.astype(jnp.bfloat16).astype(jnp.float32)
            tail = jnp.where(
                lane == sq_lane,
                high,
                jnp.where(lane == sq_lane + 1, squares - high, tail),
            )
            pout[q, d, :, 0:full] = main_g.astype(jnp.bfloat16)
            pout[q, d, :, full : 2 * full] = main_v.astype(jnp.bfloat16)
            pout[q, d, :, 2 * full : 2 * full + LANES] = tail.astype(jnp.bfloat16)
            part_copy(q, d, ahead).start()

        def pieces(ref):
            return (
                ref[q, d, :, 0:full].astype(jnp.float32),
                ref[q, d, :, full : 2 * full].astype(jnp.float32),
                ref[q, d, :, 2 * full : 2 * full + LANES].astype(jnp.float32),
            )

        @pl.when(first)
        def _():
            send(*pieces(own))

        @pl.when(jnp.logical_not(first))
        def _():
            part_copy(q, d, behind).wait_recv()
            summed = tuple(a + b for a, b in zip(pieces(own), pieces(pin)))

            @pl.when(last)
            def _():
                finish(l, q, d, *summed)
                hid_copy(q, d, behind).start()

            @pl.when(jnp.logical_not(last))
            def _():
                send(*summed)

    def spread_back(d, l, q):
        source = z + 1 if d == 0 else z - 1
        onward = z - 1 if d == 0 else z + 1
        last = (z == 0) if d == 0 else (z == R - 1)
        hid_copy(q, d, source).wait_recv()

        @pl.when(jnp.logical_not(last))
        def _():
            hid_copy(q, d, onward).start()

    def peer_copy(src, dst, send_sem, recv_sem, peer):
        return pltpu.make_async_remote_copy(
            src_ref=src,
            dst_ref=dst,
            send_sem=send_sem,
            recv_sem=recv_sem,
            device_id={"cb": peer},
            device_id_type=MESH,
        )

    def wait_group(ref, q, sem):
        view = ref.at[q, 0 : N - 1]
        pltpu.make_async_copy(view, view, sem).wait()

    def down_and_scatter(l, i, q):
        h = hid[q].reshape(rows, wide)
        product = jnp.dot(h, wd[l], preferred_element_type=jnp.float32)
        ro[q] = product.reshape(N, own_rows, Dl).astype(jnp.bfloat16)
        for k in range(1, N):
            peer = lax.rem(me + k, N)
            peer_copy(
                ro.at[q, peer], ri.at[q, me], rs_s.at[q], rs_r.at[q], peer
            ).start()
        ri[q, me] = ro[q, me]

    def sum_and_gather(l, i, q):
        wait_group(ri, q, rs_r.at[q])
        total = ri[q, 0].astype(jnp.float32)
        for k in range(1, N):
            total = total + ri[q, k].astype(jnp.float32)
        branch = total * ds_ref[pl.ds(l, 1), :]
        fresh = RESIDUAL_KEEP * xs[q, me].astype(jnp.float32) + branch
        xs[q + n, me] = fresh.astype(jnp.bfloat16)
        for k in range(1, N):
            peer = lax.rem(me + k, N)
            peer_copy(
                xs.at[q + n, me], xs.at[q + n, me], ag_s.at[q], ag_r.at[q], peer
            ).start()

    def gathered(l, i, q):
        wait_group(xs, q + n, ag_r.at[q])

        @pl.when(l == L - 1)
        def _():
            block = xs[q + n].astype(jnp.float32).reshape(rows, Dl)
            at = pl.ds(pl.multiple_of(i * rows, rows), rows)
            out_ref[at, :] = block.astype(jnp.bfloat16)

    def products(l, i, q):
        x = xs[q].astype(jnp.float32).reshape(rows, Dl)
        squares = jnp.sum(x * x, axis=1, keepdims=True)
        normed = (x * gain_ref[pl.ds(l, 1), :]).astype(jnp.bfloat16)
        result = jnp.dot(normed, wc[l], preferred_element_type=jnp.float32)
        tail_lane = lax.broadcasted_iota(jnp.int32, (rows, LANES), 1)
        tail = jnp.where(tail_lane == sq_lane, squares, result[:, 2 * full :])
        for d in range(2):
            part = slice(d * m, (d + 1) * m)
            own[q, d, :, 0 : 2 * full] = result[part, 0 : 2 * full]
            own[q, d, :, 2 * full :] = tail[part]

    def slot(t, carry):
        when_item(t - 1 - z, lambda l, i, q: chain(0, l, q))
        when_item(t - R + z, lambda l, i, q: chain(1, l, q))

        @pl.when(z < R - 1)
        def _():
            when_item(t - 2 * R + 1 + z, lambda l, i, q: spread_back(0, l, q))

        @pl.when(z > 0)
        def _():
            when_item(t - R - z, lambda l, i, q: spread_back(1, l, q))

        when_item(t - 2 * R + 1, down_and_scatter)
        for l in range(1, L):

            @pl.when(t == l * S - 5)
            def _(l=l):
                cast_weights(l)

        when_item(t - 2 * R, gathered)
        when_item(t, products)
        when_item(t - 2 * R + 1, sum_and_gather)
        return carry

    lax.fori_loop(0, (L - 1) * S + n + 2 * R, slot, 0)

    def drain(q, carry):
        @pl.when(z < R - 1)
        def _():
            part_copy(q, 0, z + 1).wait_send()
            hid_copy(q, 1, z + 1).wait_send()

        @pl.when(z > 0)
        def _():
            part_copy(q, 1, z - 1).wait_send()
            hid_copy(q, 0, z - 1).wait_send()

        wait_group(ro, q, rs_s.at[q])
        wait_group(xs, q + n, ag_s.at[q])
        return carry

    lax.fori_loop(0, L * n, drain, 0)


def solution(mesh):
    R, N = mesh.shape["ra"], mesh.shape["cb"]

    def shards(*args):
        tokens, gw, gc = args[0], args[2], args[6]
        T, Dl = tokens.shape
        L, _, F = gw.shape
        m = 32
        rows = 2 * m
        n = T // rows
        full = F // LANES * LANES
        wide = full + LANES
        packed = 2 * full + LANES
        cfg = (R, N, L, n, m, Dl * R, F)
        Q = L * n
        bf16, f32 = jnp.bfloat16, jnp.float32
        dma = pltpu.SemaphoreType.DMA
        vmem = pl.BlockSpec(memory_space=pltpu.VMEM)
        hbm = pl.BlockSpec(memory_space=pl.ANY)
        in_specs = [hbm if k in (2, 4, 10) else vmem for k in range(12)]
        return pl.pallas_call(
            functools.partial(kernel, cfg),
            out_shape=jax.ShapeDtypeStruct((T, Dl), bf16),
            in_specs=in_specs,
            out_specs=vmem,
            scratch_shapes=[
                pltpu.VMEM((Dl, F), f32),
                pltpu.VMEM((Dl, F), f32),
                pltpu.VMEM((F, Dl), f32),
                pltpu.VMEM((L, Dl, packed), bf16),
                pltpu.VMEM((L, wide, Dl), bf16),
                pltpu.VMEM((L, 16, wide), f32),
                pltpu.VMEM((Q + n, N, rows // N, Dl), bf16),
                pltpu.VMEM((Q, 2, m, packed), f32),
                pltpu.VMEM((Q, 2, m, packed), bf16),
                pltpu.VMEM((Q, 2, m, packed), bf16),
                pltpu.VMEM((Q, 2, m, wide), bf16),
                pltpu.VMEM((Q, N, rows // N, Dl), bf16),
                pltpu.VMEM((Q, N, rows // N, Dl), bf16),
                dma((3,)),
                dma((Q, 2)),
                dma((Q, 2)),
                dma((Q, 2)),
                dma((Q, 2)),
                dma((Q,)),
                dma((Q,)),
                dma((Q,)),
                dma((Q,)),
            ],
            compiler_params=pltpu.CompilerParams(
                collective_id=0,
                has_side_effects=True,
                vmem_limit_bytes=67043328,
            ),
        )(*args)

    placed = (
        P(None, "ra"),
        P(None, "ra"),
        P(None, "ra", "cb"),
        P(None, "cb"),
        P(None, "ra", "cb"),
        P(None, "cb"),
        P(None, None, "cb"),
        P(None, None, "cb"),
        P(None, "cb"),
        P(None, "cb"),
        P(None, "cb", "ra"),
        P(None, "ra"),
    )
    return jax.shard_map(
        shards, mesh=mesh, in_specs=placed, out_specs=P(None, "ra"), check_vma=False
    )
```

time: 336 us -> 150 us (0.45)
  waiting for transfers between devices: 241 us -> 0 us
  Pallas kernels: 0 us -> 130 us
  blocking collectives: 26 us -> 0 us
  other arithmetic: 22.3 us -> 0 us
  matrix products: 18 us -> 0 us
  between operations: 14.3 us -> 0.01 us
  local copies, waits for them, and re-layouts: 13.7 us -> 20 us
    pallas_call x0 -> x1, Pallas kernels: none -> 130 us  [shards(): pl.pallas_call(functools.partial(kernel, cfg), out_shape=jax.ShapeDtypeSt...]
    psum x2 -> x0, waiting for transfers between devices: 110 us -> none  [shards(): lax.psum(partial_value.astype(jnp.bfloat16), 'cb').astype(jnp.float32)]
    reduce_scatter x4 -> x0, waiting for transfers between devices: 77.5 us -> none  [the longest x2 41.5 us: shards(): lax.psum_scatter(value_part.astype(jnp.bfloat16), 'ra', scatter_dimension...]
    all_gather x2 -> x0, waiting for transfers between devices: 53.1 us -> none  [shards(): hidden = lax.all_gather(hidden, 'ra', axis=0, tiled=True)]
    unnamed x2 -> x0, blocking collectives: 26 us -> none
    dot_general x6 -> x0, matrix products: 18 us -> none  [the longest x2 7.18 us: shards(): jnp.dot(hidden, down_weight[depth_index].astype(jnp.bfloat16), preferred_...]
    another operation x3 -> x0, other arithmetic: 11.3 us -> none
    unnamed x31 -> x5, local copies, waits for them, and re-layouts: 12.7 us -> 20 us
  transfers between devices with their start and end apart: 8 -> 0, of which waited for: 8 -> 0; matrix products, arithmetic and copies ran while one was open for 6% -> 0% of each run, Pallas kernels for 0% -> 0%
where the time goes in v1:
time: 150 us
  Pallas kernels  130 us (87%)
  local copies, waits for them, and re-layouts  20 us (13%)
    pallas_call x1, Pallas kernels, shards(): pl.pallas_call(functools.partial(kernel, cfg), out_shape=jax.ShapeDtypeSt...  130 us
    unnamed x5, local copies, waits for them, and re-layouts  20 us

profile of v1, /device:TPU:0, one launch (start us, length us, event | category | flops | bytes accessed | tf_op | source)
XLA Modules:
  0.0 149.8 jit_solution(17236862822846013287)
XLA Ops:
  0.0 1.4 copy.15.gc_ref
  1.4 1.4 copy.16.vc_ref
  2.7 7.6 %copy.13.gw_ref = f32[2,768,1056]{2,1,0:T(8,128)} copy(f32[2,768,1056]{1,2,0:T(8,128)} %param.14) | data formatting | bytes 12976128 | tf_op args[2]
  10.3 7.6 %copy.14.vw_ref = f32[2,768,1056]{2,1,0:T(8,128)} copy(f32[2,768,1056]{1,2,0:T(8,128)} %param.16) | data formatting | bytes 12976128 | tf_op args[4]
  17.9 129.8 %shard_map.118 = bf16[512,768]{1,0:T(8,128)(2,1)} custom-call(bf16[512,768]{1,0:T(8,128)(2,1)} %tokens_ref.1, f32[2,768]{1,0:T(2,128)} %gain_ref.1, f32[2,768,1056]{2,1,0:T(8,128)} %copy.13.gw_ref, f32[2,1056]{1,0:T(2,128)} %gs_ref.1, f32[2,768,1056]{2,1,0:T(8,128)} %copy.14.vw_ref, f32[2,1056]{1,0:T(2,128)} %vs_ref.1, f32[2,3,1056]{2,1,0:T(4,128)} %copy.15.gc_ref, ...), custom_call_target="tpu_custom_call" | custom-call | tf_op jit(solution)/shard_map/pallas_call | solution.py:378
  147.7 2.1 %copy.18 = bf16[512,768]{1,0:T(8,128)(2,1)} copy(bf16[512,768]{1,0:T(8,128)(2,1)} %shard_map.118) | data formatting | bytes 1572864

commit v2 on v1

--- a/solution.py
+++ b/solution.py
@@ -55,7 +55,7 @@
     Dl = tokens_ref.shape[1]
     rows = 2 * m
     own_rows = rows // N
-    taps = gc_ref.shape[1]
+    taps = gc_ref.shape[0]
     full = F // LANES * LANES
     rest = F - full
     wide = full + LANES
@@ -64,15 +64,12 @@
     z = lax.axis_index("ra")
     me = lax.axis_index("cb")
 
-    def weight_copies(l):
-        return (
-            pltpu.make_async_copy(gw_ref.at[l], stage_g, w_sem.at[0]),
-            pltpu.make_async_copy(vw_ref.at[l], stage_v, w_sem.at[1]),
-            pltpu.make_async_copy(dw_ref.at[l], stage_d, w_sem.at[2]),
-        )
-
-    for copy in weight_copies(0):
-        copy.start()
+    def weight_copy(l, k):
+        src, dst = ((gw_ref, stage_g), (vw_ref, stage_v), (dw_ref, stage_d))[k]
+        return pltpu.make_async_copy(src.at[l], dst, w_sem.at[k])
+
+    for k in range(3):
+        weight_copy(0, k).start()
 
     barrier = pltpu.get_barrier_semaphore()
     for k in range(1, N):
@@ -98,44 +95,39 @@
         par[l, 1:2, 0:F] = vs_ref[l : l + 1, :]
         par[l, 2:3, 0:F] = gb_ref[l : l + 1, :]
         par[l, 3:4, 0:F] = vb_ref[l : l + 1, :]
-        par[l, 4 : 4 + taps, 0:F] = gc_ref[l]
-        par[l, 4 + taps : 4 + 2 * taps, 0:F] = vc_ref[l]
-
-    def cast_weights(l):
-        copies = weight_copies(l)
-        copies[0].wait()
-        copies[1].wait()
-
-        def up(b, carry):
-            at = pl.ds(pl.multiple_of(b * 32, 32), 32)
-            wc[l, at, 0:full] = stage_g[at, 0:full].astype(jnp.bfloat16)
-            wc[l, at, full : 2 * full] = stage_v[at, 0:full].astype(jnp.bfloat16)
-            tail = jnp.concatenate(
-                [
-                    stage_g[at, full:F],
-                    stage_v[at, full:F],
-                    jnp.zeros((32, LANES - 2 * rest), jnp.float32),
-                ],
-                axis=1,
-            )
-            wc[l, at, 2 * full : 2 * full + LANES] = tail.astype(jnp.bfloat16)
+        for k in range(taps):
+            par[l, 4 + k : 5 + k, 0:F] = gc_ref[k, l : l + 1, :]
+            par[l, 4 + taps + k : 5 + taps + k, 0:F] = vc_ref[k, l : l + 1, :]
+
+    def cast_rows(dst, l, first, src, start, count, step):
+        def move(b, carry):
+            to = pl.ds(pl.multiple_of(first + b * step, step), step)
+            at = pl.ds(pl.multiple_of(start + b * step, step), step)
+            dst[l, to, :] = src[at, :].astype(jnp.bfloat16)
             return carry
 
-        lax.fori_loop(0, Dl // 32, up, 0)
-        copies[2].wait()
-
-        def down(b, carry):
-            at = pl.ds(pl.multiple_of(b * 32, 32), 32)
-            wd[l, at, :] = stage_d[at, :].astype(jnp.bfloat16)
-            return carry
-
-        lax.fori_loop(0, F // 32, down, 0)
+        lax.fori_loop(0, count // step, move, 0)
+
+    def cast_up(l):
+        weight_copy(l, 0).wait()
+        cast_rows(wc, l, 0, stage_g, 0, full, 64)
+        cast_rows(wc, l, 2 * full, stage_g, full, rest, 32)
+        weight_copy(l, 1).wait()
+        cast_rows(wc, l, full, stage_v, 0, full, 64)
+        cast_rows(wc, l, 2 * full + rest, stage_v, full, rest, 32)
+        wc[l, 2 * F :, :] = jnp.zeros((wc.shape[1] - 2 * F, Dl), jnp.bfloat16)
+        if l + 1 < L:
+            weight_copy(l + 1, 0).start()
+            weight_copy(l + 1, 1).start()
+
+    def cast_down(l):
+        weight_copy(l, 2).wait()
+        cast_rows(wd, l, 0, stage_d, 0, F, 32)
         wd[l, F:wide, :] = jnp.zeros((wide - F, Dl), jnp.bfloat16)
-
-    cast_weights(0)
-    for l in range(1, L):
-        for copy in weight_copies(l):
-            copy.start()
+        if l + 1 < L:
+            weight_copy(l + 1, 2).start()
+
+    cast_up(0)
 
     expected = N - 1 + jnp.where(z > 0, 1, 0) + jnp.where(z < R - 1, 1, 0)
     pl.semaphore_wait(barrier, expected)
@@ -303,7 +295,12 @@
         x = xs[q].astype(jnp.float32).reshape(rows, Dl)
         squares = jnp.sum(x * x, axis=1, keepdims=True)
         normed = (x * gain_ref[pl.ds(l, 1), :]).astype(jnp.bfloat16)
-        result = jnp.dot(normed, wc[l], preferred_element_type=jnp.float32)
+        result = lax.dot_general(
+            normed,
+            wc[l],
+            (((1,), (1,)), ((), ())),
+            preferred_element_type=jnp.float32,
+        )
         tail_lane = lax.broadcasted_iota(jnp.int32, (rows, LANES), 1)
         tail = jnp.where(tail_lane == sq_lane, squares, result[:, 2 * full :])
         for d in range(2):
@@ -324,11 +321,10 @@
             when_item(t - R - z, lambda l, i, q: spread_back(1, l, q))
 
         when_item(t - 2 * R + 1, down_and_scatter)
-        for l in range(1, L):
-
-            @pl.when(t == l * S - 5)
-            def _(l=l):
-                cast_weights(l)
+        for l in range(L):
+            if l:
+                pl.when(t == l * S - 4)(functools.partial(cast_up, l))
+            pl.when(t == l * S + 1)(functools.partial(cast_down, l))
 
         when_item(t - 2 * R, gathered)
         when_item(t, products)
@@ -359,9 +355,14 @@
     R, N = mesh.shape["ra"], mesh.shape["cb"]
 
     def shards(*args):
-        tokens, gw, gc = args[0], args[2], args[6]
+        args = list(args)
+        for k in (2, 4):
+            args[k] = jnp.swapaxes(args[k], 1, 2)
+        for k in (6, 7):
+            args[k] = jnp.swapaxes(args[k], 0, 1)
+        tokens, gw = args[0], args[2]
         T, Dl = tokens.shape
-        L, _, F = gw.shape
+        L, F, _ = gw.shape
         m = 32
         rows = 2 * m
         n = T // rows
@@ -381,10 +382,10 @@
             in_specs=in_specs,
             out_specs=vmem,
             scratch_shapes=[
-                pltpu.VMEM((Dl, F), f32),
-                pltpu.VMEM((Dl, F), f32),
                 pltpu.VMEM((F, Dl), f32),
-                pltpu.VMEM((L, Dl, packed), bf16),
+                pltpu.VMEM((F, Dl), f32),
+                pltpu.VMEM((F, Dl), f32),
+                pltpu.VMEM((L, packed, Dl), bf16),
                 pltpu.VMEM((L, wide, Dl), bf16),
                 pltpu.VMEM((L, 16, wide), f32),
                 pltpu.VMEM((Q + n, N, rows // N, Dl), bf16),

time: 150 us -> 129 us (0.86)
  local copies, waits for them, and re-layouts: 20 us -> 2.06 us
  Pallas kernels: 130 us -> 127 us
    unnamed x5 -> x1, local copies, waits for them, and re-layouts: 20 us -> 2.06 us
    pallas_call x1, Pallas kernels: 130 us -> 127 us  [shards(): pl.pallas_call(functools.partial(kernel, cfg), out_shape=jax.ShapeDtypeSt...]
where the time goes in v2:
time: 129 us
  Pallas kernels  127 us (98%)
  local copies, waits for them, and re-layouts  2.06 us (2%)
    pallas_call x1, Pallas kernels, shards(): pl.pallas_call(functools.partial(kernel, cfg), out_shape=jax.ShapeDtypeSt...  127 us

profile of v2, /device:TPU:0, one launch (start us, length us, event | category | flops | bytes accessed | tf_op | source)
XLA Modules:
  0.0 129.2 jit_solution(10444062970384586826)
XLA Ops:
  0.0 127.2 %shard_map.118 = bf16[512,768]{1,0:T(8,128)(2,1)} custom-call(bf16[512,768]{1,0:T(8,128)(2,1)} %tokens_ref.1, f32[2,768]{1,0:T(2,128)} %gain_ref.1, f32[2,1056,768]{2,1,0:T(8,128)} %bitcast.4, f32[2,1056]{1,0:T(2,128)} %gs_ref.1, f32[2,1056,768]{2,1,0:T(8,128)} %bitcast.5, f32[2,1056]{1,0:T(2,128)} %vs_ref.1, f32[3,2,1056]{2,1,0:T(2,128)} %bitcast.6, ...), custom_call_target="tpu_custom_call" | custom-call | tf_op jit(solution)/shard_map/pallas_call | solution.py:379
  127.2 2.1 %copy.14 = bf16[512,768]{1,0:T(8,128)(2,1)} copy(bf16[512,768]{1,0:T(8,128)(2,1)} %shard_map.118) | data formatting | bytes 1572864
